TPU v7x, 32 devices: a whole 2x2x4 slice. The times are simulated.
32 devices in a mesh: grp: 1, ep: 16 (over z, y, x), tp: 2 (over core).
Axes of the slice: x: 2, y: 2, z: 4, core: 2. Of those that a mesh axis runs over, the one named last changes fastest.
Arguments:
- tokens: bfloat16 [512, 2048], P(('grp', 'ep')), may hold values from -6 to 6
- in_gain: bfloat16 [2048], replicated, may hold values from 0.099609375 to 1.8984375
- route_expert: int32 [512, 6], P(('grp', 'ep')), may hold values from 0 to 15, all different within a row; in each aligned block of 32 rows (0 to 31, 32 to 63, ...) at most 16 rows name the same one
- route_weight: float32 [512, 6], P(('grp', 'ep')), may hold values from 0.05 to 1
- gate_weight: bfloat16 [16, 2048, 768], P('ep', None, 'tp'), may hold values from -0.125 to 0.125
- up_weight: bfloat16 [16, 2048, 768], P('ep', None, 'tp'), may hold values from -0.125 to 0.125
- down_weight: bfloat16 [16, 768, 2048], P('ep', 'tp'), may hold values from -1 to 1
- shared_gate: bfloat16 [2048, 768], P(None, 'tp'), may hold values from -0.125 to 0.125
- shared_up: bfloat16 [2048, 768], P(None, 'tp'), may hold values from -0.125 to 0.125
- shared_down: bfloat16 [768, 2048], P('tp'), may hold values from -1 to 1
- out_gain: bfloat16 [2048], P('tp'), may hold values from 0.099609375 to 1.8984375
Outputs:
- mixed: bfloat16 [512, 2048], P(('grp', 'ep'), 'tp')
Inputs may be any that keep to these rules, and one draw needn't show every extreme that they name: `route_expert`: each row names 6 different experts. Among the rows of one device no expert is named more than 16 times, a bound that some block reaches.
All inputs are finite; a program needn't handle non-finite values.
Results may differ from a plain program's by a relative error of at most 0.0077.
Values may be sent and summed in bfloat16 or wider, within the bound.
A program may use at most 64 MiB of HBM per device.

v0:
```python
import jax
import jax.numpy as jnp
from jax import lax
from jax.sharding import PartitionSpec as P

EPSILON = 1e-06


def normalize(values, gain_vector):
    floats = values.astype(jnp.float32)
    scaled = floats * lax.rsqrt(jnp.mean(floats * floats, axis=-1, keepdims=True) + EPSILON)
    return (scaled * gain_vector.astype(jnp.float32)).astype(jnp.bfloat16)


def swiglu_hidden(inputs, gate_here, up_here):
    gate_value = jnp.dot(inputs, gate_here, preferred_element_type=jnp.float32)
    upward = jnp.dot(inputs, up_here, preferred_element_type=jnp.float32)
    return (jax.nn.silu(gate_value) * upward).astype(jnp.bfloat16)


def slot_tables(routes_here, experts, capacity):
    picked_count = routes_here.shape[0] * routes_here.shape[1]
    flattened = routes_here.reshape(picked_count)
    onehot = (flattened[:, None] == jnp.arange(experts, dtype=jnp.int32)[None, :]).astype(jnp.int32)
    earlier = jnp.cumsum(onehot, axis=0) - onehot
    ranked = jnp.sum(earlier * onehot, axis=1)
    slot_index = flattened * capacity + ranked
    source_token = jnp.arange(picked_count, dtype=jnp.int32) // routes_here.shape[1]
    matches = slot_index[None, :] == jnp.arange(experts * capacity, dtype=jnp.int32)[:, None]
    filled = jnp.any(matches, axis=1)
    slot_owner = jnp.sum(jnp.where(matches, source_token[None, :], 0), axis=1)
    return (slot_index, filled, slot_owner)


def body(
    tokens,
    in_gain,
    route_expert,
    route_weight,
    gate_weight,
    up_weight,
    down_weight,
    shared_gate,
    shared_up,
    shared_down,
    out_gain,
):
    experts = lax.axis_size("ep")
    local_tokens, model_width = tokens.shape
    top_count = route_expert.shape[1]
    capacity = max(2, (local_tokens * top_count * 4 + 3 * experts - 1) // (3 * experts))
    normed = normalize(tokens, in_gain)
    slot_index, filled, slot_owner = slot_tables(route_expert, experts, capacity)
    outgoing = jnp.where(filled[:, None], normed[slot_owner], jnp.zeros((), jnp.bfloat16))
    outgoing = outgoing.reshape(experts, capacity, model_width)
    half_width = model_width // lax.axis_size("tp")
    own_half = lax.dynamic_slice_in_dim(outgoing, lax.axis_index("tp") * half_width, half_width, 2)
    arrived = lax.all_to_all(own_half, "ep", split_axis=0, concat_axis=0, tiled=True)
    arrived = lax.all_gather(arrived, "tp", axis=2, tiled=True)
    expert_rows = arrived.reshape(experts * capacity, model_width)
    expert_part = jnp.dot(
        swiglu_hidden(expert_rows, gate_weight[0], up_weight[0]),
        down_weight[0],
        preferred_element_type=jnp.float32,
    )
    shared_part = jnp.dot(
        swiglu_hidden(normed, shared_gate, shared_up),
        shared_down,
        preferred_element_type=jnp.float32,
    )
    summed = lax.psum_scatter(
        jnp.concatenate([expert_part, shared_part], axis=0).astype(jnp.bfloat16),
        "tp",
        scatter_dimension=1,
        tiled=True,
    )
    result_rows = summed[: experts * capacity].reshape(experts, capacity, summed.shape[1])
    shared_rows = summed[experts * capacity :].astype(jnp.float32)
    returned = lax.all_to_all(result_rows, "ep", split_axis=0, concat_axis=0, tiled=True)
    returned = returned.reshape(experts * capacity, summed.shape[1])
    picked = (
        returned[slot_index].astype(jnp.float32)
        * route_weight.reshape(local_tokens * top_count)[:, None]
    )
    combined = shared_rows + jnp.sum(
        picked.reshape(local_tokens, top_count, summed.shape[1]), axis=1
    )
    squares = lax.psum(jnp.sum(combined * combined, axis=1), "tp")
    scaled = combined * lax.rsqrt(squares / model_width + EPSILON)[:, None]
    return (scaled * out_gain.astype(jnp.float32)).astype(jnp.bfloat16)


def solution(mesh):
    return jax.shard_map(
        body,
        mesh=mesh,
        in_specs=(
            P(("grp", "ep"), None),
            P(),
            P(("grp", "ep"), None),
            P(("grp", "ep"), None),
            P("ep", None, "tp"),
            P("ep", None, "tp"),
            P("ep", "tp", None),
            P(None, "tp"),
            P(None, "tp"),
            P("tp", None),
            P("tp"),
        ),
        out_specs=P(("grp", "ep"), "tp"),
        check_vma=False,
    )
```

profile of v0, /device:TPU:1, one launch (start us, length us, event | category | flops | bytes accessed | tf_op | source)
XLA Modules:
  0.0 98.1 jit_solution(16078634819476985311)
XLA Ops:
  6.5 0.0 copy-start
  6.5 0.0 all-gather.2.cloned.1.call-start
  6.5 0.9 copy.18
  7.4 0.1 reshape.115
  7.6 0.6 reduce-window.6
  8.1 0.2 slice_reduce_fusion
  8.4 0.1 bitcast_bitcast_fusion
  8.5 0.1 fusion.23
  8.6 0.1 select_reduce_fusion
  8.8 0.7 convert_element_type.38
  9.5 1.0 %fusion.19 = f32[32]{0:T(128)S(1)} fusion(bf16[32,2048]{1,0:T(8,128)(2,1)} %param.11), kind=kLoop, calls=%fused_computation.23 | loop fusion | flops 196576 | bytes 131200 | tf_op jit(solution)/shard_map/reduce_sum | solution.py:11
  10.5 0.1 broadcast_in_dim.26
  10.6 1.0 %fusion.21 = bf16[32,2048]{1,0:T(8,128)(2,1)S(1)} fusion(bf16[32,2048]{1,0:T(8,128)(2,1)} %param.11, f32[2048]{0:T(1024)S(1)} %convert_element_type.38, f32[32]{0:T(128)S(1)} %add_rsqrt_fusion.1), kind=kLoop, calls=%fused_computation.25 | loop fusion | flops 262144 | bytes 270464 | tf_op jit(solution)/shard_map/convert_element_type | solution.py:12
  11.6 1.4 %gather_fusion = bf16[256,2048]{1,0:T(8,128)(2,1)S(1)} fusion(bf16[32,2048]{1,0:T(8,128)(2,1)S(1)} %fusion.21, s32[1024]{0:T(1024)S(1)} %pad_clamp_fusion.1), kind=kCustom, calls=%fused_computation | custom fusion | bytes 2098176 | tf_op jit(solution)/shard_map/gather | solution.py:54
  13.0 0.2 dynamic-slice_select_fusion
  13.1 0.0 copy-start.2
  13.2 19.8 %all_to_all.10 = bf16[16,16,1024]{2,1,0:T(8,128)(2,1)} all-to-all(bf16[16,16,1024]{2,1,0:T(8,128)(2,1)S(1)} %dynamic-slice_select_fusion), channel_id=1, replica_groups=mesh['grp'=1,'ep'=16,'tp'=2] {'ep'}, dimensions={0} | all-to-all | bytes 1048576 | tf_op jit(solution)/shard_map/all_to_all | solution.py:58
  32.9 0.0 all-gather.2.cloned.1.call-update
  32.9 0.0 reduce-scatter.2.cloned.1.call-start
  33.0 0.0 copy-done.2
  33.0 0.3 fusion.34
  33.3 0.0 copy-start.1
  33.4 2.8 %convolution_convert_fusion.1 = bf16[32,2048]{1,0:T(8,128)(2,1)S(1)} fusion(bf16[384,2048]{1,0:T(8,128)(2,1)} %param.20, bf16[32,2048]{1,0:T(8,128)(2,1)S(1)} %fusion.21, bf16[2048,384]{1,0:T(8,128)(2,1)} %param.19, f32[32,384]{1,0:T(8,128)S(1)} %fusion.34), kind=kOutput, calls=%fused_computation.3 | convolution fusion | flops 100802560 | bytes 3457024 | tf_op jit(solution)/shard_map/dot_general | solution.py:66
  36.1 7.8 %all-gather.2.cloned.1.call-done = bf16[16,16,2048]{2,1,0:T(8,128)(2,1)} async-done(((bf16[16,16,1024]{2,1,0:T(8,128)(2,1)}), bf16[16,16,2048]{2,1,0:T(8,128)(2,1)}) %all-gather.2.cloned.1.call-update) | async-done | bytes 1048592 | tf_op jit(solution)/shard_map/all_gather | solution.py:59
  43.9 0.0 copy-done.1
  43.9 2.7 %fusion.3 = f32[256,384]{1,0:T(8,128)} fusion(bf16[256,2048]{1,0:T(8,128)(2,1)} %bitcast.44, bf16[1,2048,384]{2,1,0:T(8,128)(2,1)S(1)} %copy-done.1), kind=kOutput, calls=%fused_computation.7 | convolution fusion | flops 402653184 | bytes 3014656 | tf_op jit(solution)/shard_map/dot_general | solution.py:16
  46.6 0.0 copy-done
  46.6 3.1 %convolution_convert_fusion = bf16[256,2048]{1,0:T(8,128)(2,1)S(1)} fusion(bf16[1,384,2048]{2,1,0:T(8,128)(2,1)S(1)} %copy-done, bf16[256,2048]{1,0:T(8,128)(2,1)} %bitcast.45, bf16[1,2048,384]{2,1,0:T(8,128)(2,1)} %param.16, f32[256,384]{1,0:T(8,128)} %fusion.3), kind=kOutput, calls=%fused_computation.2 | convolution fusion | flops 806420480 | bytes 5636096 | tf_op jit(solution)/shard_map/dot_general | solution.py:61
  49.7 1.1 %pad_maximum_fusion = bf16[288,2048]{1,0:T(8,128)(2,1)} fusion(bf16[32,2048]{1,0:T(8,128)(2,1)S(1)} %convolution_convert_fusion.1, bf16[256,2048]{1,0:T(8,128)(2,1)S(1)} %convolution_convert_fusion), kind=kLoop, calls=%fused_computation.10 | loop fusion | flops 2359296 | bytes 2359296 | tf_op jit(solution)/shard_map/concatenate | solution.py:72
  50.8 0.0 copy-start.3
  50.8 0.0 copy-start.4
  50.8 0.0 reduce-scatter.2.cloned.1.call-update
  50.8 9.9 %reduce-scatter.2.cloned.1.call-done = bf16[288,1024]{1,0:T(8,128)(2,1)} async-done(((bf16[288,2048]{1,0:T(8,128)(2,1)}), bf16[288,1024]{1,0:T(8,128)(2,1)}) %reduce-scatter.2.cloned.1.call-update) | async-done | bytes 589840 | tf_op jit(solution)/shard_map/reduce_scatter | solution.py:71
  60.7 1.9 %slice.27 = bf16[256,1024]{1,0:T(8,128)(2,1)} slice(bf16[288,1024]{1,0:T(8,128)(2,1)} %reduce-scatter.2.cloned.1.call-done), slice={[0:256], [0:1024]} | slice | bytes 1048576 | tf_op jit(solution)/shard_map/slice | solution.py:77
  62.6 6.5 %all-to-all-start.1 = ((bf16[16,16,1024]{2,1,0:T(8,128)(2,1)}), bf16[16,16,1024]{2,1,0:T(8,128)(2,1)S(1)}, u32[]{:S(2)}, u32[]{:S(2)}) async-start(bf16[16,16,1024]{2,1,0:T(8,128)(2,1)} %bitcast.8), calls=%async_computation.2 | async-start | bytes 1048576 | tf_op jit(solution)/shard_map/all_to_all | solution.py:79
  69.1 0.0 copy-done.3
  69.1 0.1 copy.21
  69.2 0.1 mul.106
  69.3 0.0 copy-done.4
  69.3 0.1 copy.22
  69.4 0.0 copy-done.5
  69.4 12.4 %all-to-all-done.1 = bf16[16,16,1024]{2,1,0:T(8,128)(2,1)S(1)} async-done(((bf16[16,16,1024]{2,1,0:T(8,128)(2,1)}), bf16[16,16,1024]{2,1,0:T(8,128)(2,1)S(1)}, u32[]{:S(2)}, u32[]{:S(2)}) %all-to-all-start.1) | async-done | bytes 524320 | tf_op jit(solution)/shard_map/all_to_all | solution.py:79
  81.8 1.0 %gather_fusion.1 = bf16[192,1024]{1,0:T(8,128)(2,1)S(1)} fusion(bf16[256,1024]{1,0:T(8,128)(2,1)S(1)} %bitcast.42, s32[1024]{0:T(1024)S(1)} %pad_clamp_fusion), kind=kCustom, calls=%fused_computation.1 | custom fusion | bytes 787200 | tf_op jit(solution)/shard_map/gather | solution.py:82
  82.8 0.1 reshape.122
  82.9 0.4 multiply_reduce_fusion
  83.3 1.0 multiply_reduce_fusion.1
  84.3 5.4 %psum.7 = f32[32]{0:T(128)S(1)} all-reduce(f32[32]{0:T(128)S(1)} %multiply_reduce_fusion.1), channel_id=1, replica_groups=mesh['grp'=1,'ep'=16,'tp'=2] {'tp'}, use_global_device_ids=true, to_apply=%region_9.10 | all-reduce | flops 32 | bytes 256 | tf_op jit(solution)/shard_map/psum | solution.py:88
  89.8 1.6 %multiply_convert_fusion = bf16[32,1024]{1,0:T(8,128)(2,1)} fusion(f32[32,1024]{1,0:T(8,128)S(1)} %multiply_reduce_fusion, f32[1024]{0:T(1024)S(1)} %convert_element_type.45, f32[32]{0:T(128)S(1)} %add_rsqrt_fusion, bf16[288,1024]{1,0:T(8,128)(2,1)} %reduce-scatter.2.cloned.1.call-done), kind=kLoop, calls=%fused_computation.30 | loop fusion | flops 163840 | bytes 266368 | tf_op jit(solution)/shard_map/convert_element_type | solution.py:90
  (15 shorter events, 0.1 us)
Async XLA Ops:
  6.5 40.0 %copy-start = (bf16[1,384,2048]{2,1,0:T(8,128)(2,1)S(1)}, bf16[1,384,2048]{2,1,0:T(8,128)(2,1)}, u32[]{:S(2)}) copy-start(bf16[1,384,2048]{2,1,0:T(8,128)(2,1)} %param.17) | copy-start | bytes 4718596
  6.5 37.3 %all-gather.2.cloned.1.call-start = ((), (), s32[]{:S(2)}) async-start(), calls=%async_computation.3 | async-start | bytes 1572864 | tf_op jit(solution)/shard_map/all_gather | solution.py:59
  13.1 19.9 %copy-start.2 = (bf16[2048,384]{1,0:T(8,128)(2,1)S(1)}, bf16[2048,384]{1,0:T(8,128)(2,1)}, u32[]{:S(2)}) copy-start(bf16[2048,384]{1,0:T(8,128)(2,1)} %param.18) | copy-start | bytes 4718596
  32.9 27.7 %reduce-scatter.2.cloned.1.call-start = ((), (), s32[]{:S(2)}) async-start(), calls=%async_computation.4 | async-start | bytes 1769472 | tf_op jit(solution)/shard_map/reduce_scatter | solution.py:71
  33.3 10.5 %copy-start.1 = (bf16[1,2048,384]{2,1,0:T(8,128)(2,1)S(1)}, bf16[1,2048,384]{2,1,0:T(8,128)(2,1)}, u32[]{:S(2)}) copy-start(bf16[1,2048,384]{2,1,0:T(8,128)(2,1)} %param.15) | copy-start | bytes 4718596
  50.8 18.3 %copy-start.3 = (s32[32,6]{0,1:T(8,128)S(1)}, s32[32,6]{0,1:T(8,128)}, u32[]{:S(2)}) copy-start(s32[32,6]{0,1:T(8,128)} %param.13) | copy-start | bytes 2308
  50.8 18.5 %copy-start.4 = (f32[32,6]{0,1:T(8,128)S(1)}, f32[32,6]{0,1:T(8,128)}, u32[]{:S(2)}) copy-start(f32[32,6]{0,1:T(8,128)} %param.14) | copy-start | bytes 2308
  50.8 18.6 %copy-start.5 = (bf16[1024]{0:T(1024)(128)(2,1)S(1)}, bf16[1024]{0:T(1024)(128)(2,1)}, u32[]{:S(2)}) copy-start(bf16[1024]{0:T(1024)(128)(2,1)} %param.21) | copy-start | bytes 6148
  62.6 19.3 %all-to-all-start.1 = ((bf16[16,16,1024]{2,1,0:T(8,128)(2,1)}), bf16[16,16,1024]{2,1,0:T(8,128)(2,1)S(1)}, u32[]{:S(2)}, u32[]{:S(2)}) async-start(bf16[16,16,1024]{2,1,0:T(8,128)(2,1)} %bitcast.8), calls=%async_computation.2 | async-start | bytes 1048576 | tf_op jit(solution)/shard_map/all_to_all | solution.py:79
Sparse Core Ops, SparseCore 0:
  33.1 10.7 all-gather.1
  50.9 9.7 reduce-scatter.1
where the time goes:
time: 99 us; the launch traced here: 98.1 us
  waiting for transfers between devices  30.1 us (30%)
  blocking collectives  25.2 us (25%)
  between operations  13.6 us (14%)
  matrix products  8.91 us (9%)
  other arithmetic  7.94 us (8%)
  starting transfers between devices  6.57 us (7%)
  local copies, waits for them, and re-layouts  5.9 us (6%)
    all_to_all x1, blocking collectives, body(): lax.all_to_all(own_half, 'ep', split_axis=0, concat_axis=0, tiled=True)  19.8 us
    all_to_all x1, waiting for transfers between devices, body(): lax.all_to_all(result_rows, 'ep', split_axis=0, concat_axis=0, tiled=True)  12.4 us
    reduce_scatter x1, waiting for transfers between devices, body(): lax.psum_scatter(jnp.concatenate([expert_part, shared_part], axis=0).asty...  9.87 us
    all_gather x1, waiting for transfers between devices, body(): arrived = lax.all_gather(arrived, 'tp', axis=2, tiled=True)  7.76 us
    all_to_all x1, starting transfers between devices, body(): lax.all_to_all(result_rows, 'ep', split_axis=0, concat_axis=0, tiled=True)  6.53 us
    psum x1, blocking collectives, body(): squares = lax.psum(jnp.sum(combined * combined, axis=1), 'tp')  5.44 us
    dot_general x1, matrix products, body(): jnp.dot(swiglu_hidden(expert_rows, gate_weight[0], up_weight[0]), down_we...  3.14 us
    dot_general x2, matrix products, swiglu_hidden(): gate_value = jnp.dot(inputs, gate_here, preferred_element_type=jnp.float32)  3.01 us
  transfers between devices with their start and end apart: 3, of which 3 were waited for; matrix products, arithmetic and copies ran while one was open for 3% of the time, Pallas kernels for 0%

commit v1 on v0

v1 whole, which is shorter than its diff:
```python
import functools

import jax
import jax.numpy as jnp
from jax import lax
from jax.experimental import pallas as pl
from jax.experimental.pallas import tpu as pltpu
from jax.sharding import PartitionSpec as P

EPSILON = 1e-06
F32 = jnp.float32
BF16 = jnp.bfloat16


def dot(a, b):
    return jnp.dot(a, b, preferred_element_type=F32)


def dot_t(a, b):
    return lax.dot_general(a, b, (((1,), (1,)), ((), ())), preferred_element_type=F32)


def silu_product(gate_value, upward):
    return (gate_value * (1.0 / (1.0 + jnp.exp(-gate_value))) * upward).astype(BF16)


def kernel(
    outer,
    inner,
    cap,
    info_width,
    tokens,
    in_gain,
    route_expert,
    route_weight,
    out_gain,
    gate_hbm,
    up_hbm,
    down_hbm,
    sgate_hbm,
    sup_hbm,
    sdown_hbm,
    mixed,
    gate_w,
    up_w,
    down_w,
    sgate_w,
    sup_w,
    sdown_w,
    normed,
    column,
    staged,
    rows_in,
    gate_acc,
    up_acc,
    part_out,
    part_in,
    part_own,
    result,
    back,
    sum_out,
    sum_in,
    shared_out,
    shared_in,
    squares_out,
    squares_in,
    w_sem,
    col_send,
    col_recv,
    plane_send,
    plane_recv,
    pair_send,
    pair_recv,
    part_send,
    part_recv,
    shared_sem,
    back_send,
    back_recv,
    sum_send,
    sum_recv,
    sq_sem,
):
    ep = lax.axis_index("ep")
    tp = lax.axis_index("tp")
    z = ep // inner
    p = ep % inner
    other = 1 - tp
    experts = outer * inner
    local_tokens, width = tokens.shape
    half = width // 2

    loads = [
        pltpu.make_async_copy(src, dst, w_sem.at[i])
        for i, (src, dst) in enumerate(
            [
                (sgate_hbm, sgate_w),
                (sup_hbm, sup_w),
                (sdown_hbm, sdown_w),
                (gate_hbm.at[0], gate_w),
                (up_hbm.at[0], up_w),
                (down_hbm.at[0], down_w),
            ]
        )
    ]
    for load in loads:
        load.start()

    barrier = pltpu.get_barrier_semaphore()

    def greet(ep_to, tp_to):
        pl.semaphore_signal(
            barrier, inc=1, device_id={"ep": ep_to, "tp": tp_to}, device_id_type=pl.DeviceIdType.MESH
        )

    for d in range(1, outer):
        greet(lax.rem(z + d, outer) * inner + p, tp)
    for d in range(1, inner):
        greet(z * inner + lax.rem(p + d, inner), tp)
    greet(ep, other)

    def remote(src, dst, send, recv, ep_to, tp_to):
        return pltpu.make_async_remote_copy(
            src_ref=src,
            dst_ref=dst,
            send_sem=send,
            recv_sem=recv,
            device_id={"ep": ep_to, "tp": tp_to},
            device_id_type=pl.DeviceIdType.MESH,
        )

    floats = tokens[...].astype(F32)
    mean = jnp.sum(floats * floats, axis=1, keepdims=True) / width
    rows = (floats * lax.rsqrt(mean + EPSILON) * in_gain[...].astype(F32)).astype(BF16)
    normed[...] = rows

    lane = lax.broadcasted_iota(jnp.int32, (local_tokens, info_width), 1)
    lane_expert = lax.rem(lane, experts)
    named = jnp.zeros((local_tokens, info_width), F32)
    weight = jnp.zeros((local_tokens, info_width), F32)
    for k in range(route_expert.shape[1]):
        hit = route_expert[:, k : k + 1] == lane_expert
        named = named + jnp.where(hit, 1.0, 0.0)
        weight = weight + jnp.where(hit, route_weight[:, k : k + 1], 0.0)
    row_i = lax.broadcasted_iota(jnp.int32, (local_tokens, local_tokens), 0)
    col_i = lax.broadcasted_iota(jnp.int32, (local_tokens, local_tokens), 1)
    upto = jnp.where(col_i <= row_i, 1.0, 0.0).astype(BF16)
    place = dot(upto, named.astype(BF16)) * named
    high = weight.astype(BF16).astype(F32)
    info = jnp.where(lane < experts, place, jnp.where(lane < 2 * experts, high, weight - high))
    info = jnp.where(lane < 3 * experts, info, 0.0)

    @pl.when(tp == 0)
    def _():
        column[z, :, :half] = rows[:, :half]

    @pl.when(tp == 1)
    def _():
        column[z, :, :half] = rows[:, half:]

    column[z, :, half:] = info.astype(BF16)

    pl.semaphore_wait(barrier, outer + inner - 1)

    sends = []
    for d in range(1, outer):
        to = lax.rem(z + d, outer)
        copy = remote(
            column.at[z], column.at[z], col_send.at[to], col_recv.at[z], to * inner + p, tp
        )
        copy.start()
        sends.append(copy)

    slots = inner * cap
    slot_row = lax.broadcasted_iota(jnp.int32, (slots, info_width), 0)
    slot_lane = lax.broadcasted_iota(jnp.int32, (slots, info_width), 1)
    slot_expert = z * inner + slot_row // cap

    def selector(offset):
        return jnp.where(slot_lane == slot_expert + offset, 1.0, 0.0).astype(BF16)

    pick_place = selector(0)
    slot_rank = (lax.broadcasted_iota(jnp.int32, (slots, local_tokens), 0) % cap + 1).astype(F32)

    def dispatch(j):
        where = dot_t(pick_place, column[j, :, half:])
        onehot = jnp.where(where == slot_rank, 1.0, 0.0).astype(BF16)
        moved = dot(onehot, column[j, :, :half]).astype(BF16)
        staged[j] = moved.reshape(inner, cap, half)
        for d in range(1, inner):
            to = lax.rem(p + d, inner)
            copy = remote(
                staged.at[j, to],
                rows_in.at[tp, j, p],
                plane_send.at[j, to],
                plane_recv.at[j, p],
                z * inner + to,
                tp,
            )
            copy.start()
            sends.append(copy)
        rows_in[tp, j, p] = staged[j, p]

    dispatch(z)
    for d in range(1, outer):
        j = lax.rem(z + d, outer)
        remote(
            column.at[j], column.at[j], col_send.at[j], col_recv.at[j], ep, tp
        ).wait_recv()
        dispatch(j)

    for load in loads[:3]:
        load.wait()
    inputs = normed[...]
    shared_hidden = silu_product(dot(inputs, sgate_w[...]), dot(inputs, sup_w[...]))
    shared_out[...] = dot(
        shared_hidden, sdown_w[:, pl.ds(pl.multiple_of(other * half, half), half)]
    ).astype(BF16)
    shared_copy = remote(shared_out, shared_in, shared_sem.at[0], shared_sem.at[1], ep, other)
    shared_copy.start()
    shared_own = dot(shared_hidden, sdown_w[:, pl.ds(pl.multiple_of(tp * half, half), half)])

    for load in loads[3:]:
        load.wait()

    pair_copies = []
    for d in range(outer):
        j = lax.rem(z + d, outer)
        for e in range(1, inner):
            source = lax.rem(p + e, inner)
            remote(
                staged.at[j, source],
                rows_in.at[tp, j, source],
                plane_send.at[j, source],
                plane_recv.at[j, source],
                ep,
                tp,
            ).wait_recv()
        copy = remote(
            rows_in.at[tp, j], rows_in.at[tp, j], pair_send.at[j], pair_recv.at[j], ep, other
        )
        copy.start()
        pair_copies.append(copy)

    total = experts * cap

    def half_rows(which):
        return pl.ds(pl.multiple_of(which * half, half), half)

    own_rows = rows_in[tp].reshape(total, half)
    gate_acc[...] = dot(own_rows, gate_w[half_rows(tp), :])
    up_acc[...] = dot(own_rows, up_w[half_rows(tp), :])
    for d in range(outer):
        j = lax.rem(z + d, outer)
        remote(
            rows_in.at[other, j], rows_in.at[other, j], pair_send.at[j], pair_recv.at[j], ep, other
        ).wait_recv()
    other_rows = rows_in[other].reshape(total, half)
    gate_value = gate_acc[...] + dot(other_rows, gate_w[half_rows(other), :])
    upward = up_acc[...] + dot(other_rows, up_w[half_rows(other), :])
    hidden = silu_product(gate_value, upward)

    part_out[...] = (
        dot(hidden, down_w[:, half_rows(other)]).astype(BF16).reshape(outer, inner, cap, half)
    )
    for d in range(outer):
        j = lax.rem(z + 1 + d, outer)
        copy = remote(part_out.at[j], part_in.at[j], part_send.at[j], part_recv.at[j], ep, other)
        copy.start()
        sends.append(copy)
    part_own[...] = (
        dot(hidden, down_w[:, half_rows(tp)]).astype(BF16).reshape(outer, inner, cap, half)
    )

    for d in range(outer):
        j = lax.rem(z + 1 + d, outer)
        remote(
            part_out.at[j], part_in.at[j], part_send.at[j], part_recv.at[j], ep, other
        ).wait_recv()
        summed = part_own[j].astype(F32) + part_in[j].astype(F32)
        result[j] = summed.astype(BF16)
        for e in range(1, inner):
            to = lax.rem(p + e, inner)
            copy = remote(
                result.at[j, to],
                back.at[j, p],
                back_send.at[j, to],
                back_recv.at[j, p],
                z * inner + to,
                tp,
            )
            copy.start()
            sends.append(copy)
        back[j, p] = result[j, p]

    pick_high = selector(experts)
    pick_low = selector(2 * experts)
    slot_of_lane = (lax.broadcasted_iota(jnp.int32, (local_tokens, slots), 1) % cap + 1).astype(F32)

    def combine(j):
        facts = column[j, :, half:]
        chosen = dot_t(facts, pick_place) == slot_of_lane
        high_part = jnp.where(chosen, dot_t(facts, pick_high), 0.0).astype(BF16)
        low_part = jnp.where(chosen, dot_t(facts, pick_low), 0.0).astype(BF16)
        for e in range(1, inner):
            source = lax.rem(p + e, inner)
            remote(
                result.at[j, source],
                back.at[j, source],
                back_send.at[j, source],
                back_recv.at[j, source],
                ep,
                tp,
            ).wait_recv()
        values = back[j].reshape(slots, half)
        return dot(high_part, values) + dot(low_part, values)

    for d in range(1, outer):
        j = lax.rem(z + d, outer)
        sum_out[j] = combine(j).astype(BF16)
        copy = remote(
            sum_out.at[j], sum_in.at[z], sum_send.at[j], sum_recv.at[z], j * inner + p, tp
        )
        copy.start()
        sends.append(copy)
    combined = combine(z)
    shared_copy.wait_recv()
    combined = combined + (
        shared_own.astype(BF16).astype(F32) + shared_in[...].astype(F32)
    ).astype(BF16).astype(F32)
    for d in range(1, outer):
        j = lax.rem(z + d, outer)
        remote(
            sum_out.at[j], sum_in.at[j], sum_send.at[j], sum_recv.at[j], ep, tp
        ).wait_recv()
        combined = combined + sum_in[j].astype(F32)

    own_squares = jnp.sum(combined * combined, axis=1, keepdims=True)
    squares_out[...] = jnp.broadcast_to(own_squares, squares_out.shape)
    sq_copy = remote(squares_out, squares_in, sq_sem.at[0], sq_sem.at[1], ep, other)
    sq_copy.start()
    sq_copy.wait_recv()
    squares = own_squares + squares_in[:, :1]
    scaled = combined * lax.rsqrt(squares / width + EPSILON)
    mixed[...] = (scaled * out_gain[...].astype(F32)).astype(BF16)

    for copy in sends:
        copy.wait_send()
    for copy in pair_copies:
        copy.wait_send()
    shared_copy.wait_send()
    sq_copy.wait_send()


def body(
    experts,
    tokens,
    in_gain,
    route_expert,
    route_weight,
    gate_weight,
    up_weight,
    down_weight,
    shared_gate,
    shared_up,
    shared_down,
    out_gain,
):
    inner = 1
    while inner * inner < experts:
        inner *= 2
    outer = experts // inner
    local_tokens, width = tokens.shape
    half = width // 2
    top_count = route_expert.shape[1]
    capacity = max(2, (local_tokens * top_count * 4 + 3 * experts - 1) // (3 * experts))
    cap = -(-capacity // 16) * 16
    info_width = -(-3 * experts // 128) * 128
    hidden = gate_weight.shape[2]
    shared_width = shared_gate.shape[1]
    total = experts * cap

    def vm(shape, kind=BF16):
        return pltpu.VMEM(shape, kind)

    grid_rows = (outer, inner, cap, half)
    dma = pltpu.SemaphoreType.DMA
    in_vmem = pl.BlockSpec(memory_space=pltpu.VMEM)
    anywhere = pl.BlockSpec(memory_space=pl.ANY)
    return pl.pallas_call(
        functools.partial(kernel, outer, inner, cap, info_width),
        out_shape=jax.ShapeDtypeStruct((local_tokens, half), BF16),
        in_specs=[in_vmem] * 5 + [anywhere] * 6,
        out_specs=in_vmem,
        scratch_shapes=[
            vm((width, hidden)),
            vm((width, hidden)),
            vm((hidden, width)),
            vm((width, shared_width)),
            vm((width, shared_width)),
            vm((shared_width, width)),
            vm((local_tokens, width)),
            vm((outer, local_tokens, half + info_width)),
            vm(grid_rows),
            vm((2,) + grid_rows),
            vm((total, hidden), F32),
            vm((total, hidden), F32),
            vm(grid_rows),
            vm(grid_rows),
            vm(grid_rows),
            vm(grid_rows),
            vm(grid_rows),
            vm((outer, local_tokens, half)),
            vm((outer, local_tokens, half)),
            vm((local_tokens, half)),
            vm((local_tokens, half)),
            vm((local_tokens, 128), F32),
            vm((local_tokens, 128), F32),
            dma((6,)),
            dma((outer,)),
            dma((outer,)),
            dma((outer, inner)),
            dma((outer, inner)),
            dma((outer,)),
            dma((outer,)),
            dma((outer,)),
            dma((outer,)),
            dma((2,)),
            dma((outer, inner)),
            dma((outer, inner)),
            dma((outer,)),
            dma((outer,)),
            dma((2,)),
        ],
        compiler_params=pltpu.CompilerParams(
            collective_id=0, has_side_effects=True, vmem_limit_bytes=60 * 1024 * 1024
        ),
    )(
        tokens,
        in_gain.reshape(1, width),
        route_expert,
        route_weight,
        out_gain.reshape(1, half),
        gate_weight,
        up_weight,
        down_weight,
        shared_gate,
        shared_up,
        shared_down,
    )


def solution(mesh):
    return jax.shard_map(
        functools.partial(body, mesh.shape["ep"]),
        mesh=mesh,
        in_specs=(
            P(("grp", "ep"), None),
            P(),
            P(("grp", "ep"), None),
            P(("grp", "ep"), None),
            P("ep", None, "tp"),
            P("ep", None, "tp"),
            P("ep", "tp", None),
            P(None, "tp"),
            P(None, "tp"),
            P("tp", None),
            P("tp"),
        ),
        out_specs=P(("grp", "ep"), "tp"),
        check_vma=False,
    )
```

time: 99 us -> 43 us (0.43)
  Pallas kernels: 0 us -> 35.9 us
  waiting for transfers between devices: 30.1 us -> 0 us
  blocking collectives: 25.2 us -> 0 us
  between operations: 13.6 us -> 0.01 us
  matrix products: 8.91 us -> 0 us
  other arithmetic: 7.94 us -> 0 us
  starting transfers between devices: 6.57 us -> 0 us
    pallas_call x0 -> x1, Pallas kernels: none -> 35.9 us  [body(): pl.pallas_call(functools.partial(kernel, outer, inner, cap, info_width),...]
    all_to_all x1 -> x0, blocking collectives: 19.8 us -> none  [body(): lax.all_to_all(own_half, 'ep', split_axis=0, concat_axis=0, tiled=True)]
    all_to_all x1 -> x0, waiting for transfers between devices: 12.4 us -> none  [body(): lax.all_to_all(result_rows, 'ep', split_axis=0, concat_axis=0, tiled=True)]
    reduce_scatter x1 -> x0, waiting for transfers between devices: 9.87 us -> none  [body(): lax.psum_scatter(jnp.concatenate([expert_part, shared_part], axis=0).asty...]
    dot_general x4 -> x0, matrix products: 8.91 us -> none  [the longest x1 3.14 us: body(): jnp.dot(swiglu_hidden(expert_rows, gate_weight[0], up_weight[0]), down_we...]
    all_gather x1 -> x0, waiting for transfers between devices: 7.76 us -> none  [body(): arrived = lax.all_gather(arrived, 'tp', axis=2, tiled=True)]
    all_to_all x1 -> x0, starting transfers between devices: 6.53 us -> none  [body(): lax.all_to_all(result_rows, 'ep', split_axis=0, concat_axis=0, tiled=True)]
    psum x1 -> x0, blocking collectives: 5.44 us -> none  [body(): squares = lax.psum(jnp.sum(combined * combined, axis=1), 'tp')]
  transfers between devices with their start and end apart: 3 -> 0, of which waited for: 3 -> 0; matrix products, arithmetic and copies ran while one was open for 3% -> 0% of each run, Pallas kernels for 0% -> 0%
where the time goes in v1:
time: 43 us; the launch traced here: 42.7 us
  Pallas kernels  35.9 us (83%)
  local copies, waits for them, and re-layouts  6.78 us (16%)
    pallas_call x1, Pallas kernels, body(): pl.pallas_call(functools.partial(kernel, outer, inner, cap, info_width),...  35.9 us
    unnamed x3, local copies, waits for them, and re-layouts  4.21 us
    reshape x1, local copies, waits for them, and re-layouts, body(): in_gain.reshape(1, width)  1.29 us
    reshape x1, local copies, waits for them, and re-layouts, body(): out_gain.reshape(1, half)  1.28 us

profile of v1, /device:TPU:1, one launch (start us, length us, event | category | flops | bytes accessed | tf_op | source)
XLA Modules:
  0.0 42.7 jit_solution(10588413716400659869)
XLA Ops:
  0.0 1.3 %reshape.7.out_gain = bf16[1,1024]{1,0:T(2,128)(2,1)} reshape(bf16[1024]{0:T(1024)(128)(2,1)} %param.21) | data formatting | bytes 4096 | tf_op jit(solution)/shard_map/reshape | solution.py:442
  1.3 1.3 %reshape.6.in_gain = bf16[1,2048]{1,0:T(2,128)(2,1)} reshape(bf16[2048]{0:T(1024)(128)(2,1)} %param.12) | data formatting | bytes 8192 | tf_op jit(solution)/shard_map/reshape | solution.py:439
  2.6 1.4 %copy.12.route_expert = s32[32,6]{1,0:T(8,128)} copy(s32[32,6]{0,1:T(8,128)} %param.13) | data formatting | bytes 1536 | tf_op args[2]
  3.9 1.4 %copy.13.route_weight = f32[32,6]{1,0:T(8,128)} copy(f32[32,6]{0,1:T(8,128)} %param.14) | data formatting | bytes 1536 | tf_op args[3]
  5.3 35.9 %shard_map.109 = bf16[32,1024]{1,0:T(8,128)(2,1)} custom-call(bf16[32,2048]{1,0:T(8,128)(2,1)} %tokens.1, bf16[1,2048]{1,0:T(2,128)(2,1)} %reshape.6.in_gain, s32[32,6]{1,0:T(8,128)} %copy.12.route_expert, f32[32,6]{1,0:T(8,128)} %copy.13.route_weight, bf16[1,1024]{1,0:T(2,128)(2,1)} %reshape.7.out_gain, bf16[1,2048,384]{2,1,0:T(8,128)(2,1)} %gate_hbm.1, ...), custom_call_target="tpu_custom_call" | custom-call | tf_op jit(solution)/shard_map/pallas_call | solution.py:389
  41.2 1.5 %copy.15 = bf16[32,1024]{1,0:T(8,128)(2,1)} copy(bf16[32,1024]{1,0:T(8,128)(2,1)} %shard_map.109) | data formatting | bytes 131072

commit v2 on v1

--- a/solution.py
+++ b/solution.py
@@ -130,24 +130,26 @@
 
     floats = tokens[...].astype(F32)
     mean = jnp.sum(floats * floats, axis=1, keepdims=True) / width
-    rows = (floats * lax.rsqrt(mean + EPSILON) * in_gain[...].astype(F32)).astype(BF16)
+    rows = (floats * lax.rsqrt(mean + EPSILON) * in_gain[...].astype(F32)[None, :]).astype(BF16)
     normed[...] = rows
 
-    lane = lax.broadcasted_iota(jnp.int32, (local_tokens, info_width), 1)
-    lane_expert = lax.rem(lane, experts)
-    named = jnp.zeros((local_tokens, info_width), F32)
-    weight = jnp.zeros((local_tokens, info_width), F32)
-    for k in range(route_expert.shape[1]):
-        hit = route_expert[:, k : k + 1] == lane_expert
+    fact = lax.broadcasted_iota(jnp.int32, (info_width, local_tokens), 0)
+    fact_expert = lax.rem(fact, experts)
+    named = jnp.zeros((info_width, local_tokens), F32)
+    weight = jnp.zeros((info_width, local_tokens), F32)
+    for k in range(route_expert.shape[0]):
+        hit = route_expert[k : k + 1, :] == fact_expert
         named = named + jnp.where(hit, 1.0, 0.0)
-        weight = weight + jnp.where(hit, route_weight[:, k : k + 1], 0.0)
+        weight = weight + jnp.where(hit, route_weight[k : k + 1, :], 0.0)
     row_i = lax.broadcasted_iota(jnp.int32, (local_tokens, local_tokens), 0)
     col_i = lax.broadcasted_iota(jnp.int32, (local_tokens, local_tokens), 1)
-    upto = jnp.where(col_i <= row_i, 1.0, 0.0).astype(BF16)
-    place = dot(upto, named.astype(BF16)) * named
+    upto = jnp.where(row_i <= col_i, 1.0, 0.0).astype(BF16)
+    place = dot(named.astype(BF16), upto) * named
     high = weight.astype(BF16).astype(F32)
-    info = jnp.where(lane < experts, place, jnp.where(lane < 2 * experts, high, weight - high))
-    info = jnp.where(lane < 3 * experts, info, 0.0)
+    facts = jnp.where(fact < experts, place, jnp.where(fact < 2 * experts, high, weight - high))
+    facts = jnp.where(fact < 3 * experts, facts, 0.0).astype(BF16)
+    same = jnp.where(row_i == col_i, 1.0, 0.0).astype(BF16)
+    info = dot_t(same, facts)
 
     @pl.when(tp == 0)
     def _():
@@ -201,12 +203,6 @@
         rows_in[tp, j, p] = staged[j, p]
 
     dispatch(z)
-    for d in range(1, outer):
-        j = lax.rem(z + d, outer)
-        remote(
-            column.at[j], column.at[j], col_send.at[j], col_recv.at[j], ep, tp
-        ).wait_recv()
-        dispatch(j)
 
     for load in loads[:3]:
         load.wait()
@@ -218,6 +214,13 @@
     shared_copy = remote(shared_out, shared_in, shared_sem.at[0], shared_sem.at[1], ep, other)
     shared_copy.start()
     shared_own = dot(shared_hidden, sdown_w[:, pl.ds(pl.multiple_of(tp * half, half), half)])
+
+    for d in range(1, outer):
+        j = lax.rem(z + d, outer)
+        remote(
+            column.at[j], column.at[j], col_send.at[j], col_recv.at[j], ep, tp
+        ).wait_recv()
+        dispatch(j)
 
     for load in loads[3:]:
         load.wait()
@@ -341,7 +344,7 @@
     sq_copy.wait_recv()
     squares = own_squares + squares_in[:, :1]
     scaled = combined * lax.rsqrt(squares / width + EPSILON)
-    mixed[...] = (scaled * out_gain[...].astype(F32)).astype(BF16)
+    mixed[...] = (scaled * out_gain[...].astype(F32)[None, :]).astype(BF16)
 
     for copy in sends:
         copy.wait_send()
@@ -436,10 +439,10 @@
         ),
     )(
         tokens,
-        in_gain.reshape(1, width),
-        route_expert,
-        route_weight,
-        out_gain.reshape(1, half),
+        in_gain,
+        route_expert.T,
+        route_weight.T,
+        out_gain,
         gate_weight,
         up_weight,
         down_weight,

time: 43 us -> 37.6 us (0.87)
  local copies, waits for them, and re-layouts: 6.78 us -> 1.47 us
    unnamed x3 -> x1, local copies, waits for them, and re-layouts: 4.21 us -> 1.47 us
    reshape x2 -> x0, local copies, waits for them, and re-layouts: 2.57 us -> none  [the longest x1 1.29 us: body(): in_gain.reshape(1, width)]
where the time goes in v2:
time: 37.6 us; the launch traced here: 37.4 us
  Pallas kernels  35.9 us (95%)
  local copies, waits for them, and re-layouts  1.47 us (4%)
    pallas_call x1, Pallas kernels, body(): pl.pallas_call(functools.partial(kernel, outer, inner, cap, info_width),...  35.9 us
    unnamed x1, local copies, waits for them, and re-layouts  1.47 us

profile of v2, /device:TPU:1, one launch (start us, length us, event | category | flops | bytes accessed | tf_op | source)
XLA Modules:
  0.0 37.4 jit_solution(2683194901498672273)
XLA Ops:
  0.0 35.9 %shard_map.109 = bf16[32,1024]{1,0:T(8,128)(2,1)} custom-call(bf16[32,2048]{1,0:T(8,128)(2,1)} %tokens.1, bf16[2048]{0:T(1024)(128)(2,1)} %in_gain.1, s32[6,32]{1,0:T(8,128)} %bitcast.2, f32[6,32]{1,0:T(8,128)} %bitcast.3, bf16[1024]{0:T(1024)(128)(2,1)} %out_gain.1, bf16[1,2048,384]{2,1,0:T(8,128)(2,1)} %gate_hbm.1, bf16[1,2048,384]{2,1,0:T(8,128)(2,1)} %up_hbm.1, ...), custom_call_target="tpu_custom_call" | custom-call | tf_op jit(solution)/shard_map/pallas_call | solution.py:392
  35.9 1.5 %copy.13 = bf16[32,1024]{1,0:T(8,128)(2,1)} copy(bf16[32,1024]{1,0:T(8,128)(2,1)} %shard_map.109) | data formatting | bytes 131072

commit v3 on v2

--- a/solution.py
+++ b/solution.py
@@ -51,8 +51,6 @@
     column,
     staged,
     rows_in,
-    gate_acc,
-    up_acc,
     part_out,
     part_in,
     part_own,
@@ -67,6 +65,7 @@
     w_sem,
     col_send,
     col_recv,
+    col_pass,
     plane_send,
     plane_recv,
     pair_send,
@@ -164,13 +163,43 @@
     pl.semaphore_wait(barrier, outer + inner - 1)
 
     sends = []
-    for d in range(1, outer):
-        to = lax.rem(z + d, outer)
-        copy = remote(
-            column.at[z], column.at[z], col_send.at[to], col_recv.at[z], to * inner + p, tp
-        )
+
+    def send(src, dst, send_sem, recv_sem, ep_to, tp_to):
+        copy = remote(src, dst, send_sem, recv_sem, ep_to, tp_to)
         copy.start()
         sends.append(copy)
+
+    def arrive(ref, send_sem, recv_sem):
+        remote(ref, ref, send_sem, recv_sem, ep, other).wait_recv()
+
+    short = jnp.minimum(z, outer - 1 - z)
+
+    def nth(i):
+        if i == 0:
+            return z
+        near = (i + 1) // 2 if i % 2 else -(i // 2)
+        far = jnp.where(z < outer - 1 - z, i - short, short - i)
+        return z + jnp.where(i <= 2 * short, near, far)
+
+    order = [nth(i) for i in range(outer)]
+
+    def column_copy(block, to, send_sem):
+        here = column.at[block]
+        return remote(here, here, send_sem, col_recv.at[block], to * inner + p, tp)
+
+    def direct(to):
+        return (to - z) * (to - z) != 4
+
+    def passes(j):
+        on = 2 * z - j
+        return on, ((j - z) * (j - z) == 1) & (on >= 0) & (on < outer)
+
+    for to in order[1:]:
+
+        @pl.when(direct(to))
+        def _(to=to):
+            column_copy(z, to, col_send.at[to]).start()
+
 
     slots = inner * cap
     slot_row = lax.broadcasted_iota(jnp.int32, (slots, info_width), 0)
@@ -181,16 +210,31 @@
         return jnp.where(slot_lane == slot_expert + offset, 1.0, 0.0).astype(BF16)
 
     pick_place = selector(0)
+    pick_high = selector(experts)
+    pick_low = selector(2 * experts)
     slot_rank = (lax.broadcasted_iota(jnp.int32, (slots, local_tokens), 0) % cap + 1).astype(F32)
-
-    def dispatch(j):
+    slot_of_lane = (lax.broadcasted_iota(jnp.int32, (local_tokens, slots), 1) % cap + 1).astype(F32)
+    peers = [lax.rem(p + e, inner) for e in range(1, inner)]
+
+    def half_of(which):
+        return pl.ds(pl.multiple_of(which * half, half), half)
+
+    def dispatch(i):
+        j = order[i]
+        if i:
+            arrive(column.at[j], col_send.at[j], col_recv.at[j])
+            on, wanted = passes(j)
+
+            @pl.when(wanted)
+            def _():
+                column_copy(j, on, col_pass.at[j]).start()
+
         where = dot_t(pick_place, column[j, :, half:])
         onehot = jnp.where(where == slot_rank, 1.0, 0.0).astype(BF16)
         moved = dot(onehot, column[j, :, :half]).astype(BF16)
         staged[j] = moved.reshape(inner, cap, half)
-        for d in range(1, inner):
-            to = lax.rem(p + d, inner)
-            copy = remote(
+        for to in peers:
+            send(
                 staged.at[j, to],
                 rows_in.at[tp, j, p],
                 plane_send.at[j, to],
@@ -198,92 +242,52 @@
                 z * inner + to,
                 tp,
             )
-            copy.start()
-            sends.append(copy)
         rows_in[tp, j, p] = staged[j, p]
 
-    dispatch(z)
-
-    for load in loads[:3]:
-        load.wait()
-    inputs = normed[...]
-    shared_hidden = silu_product(dot(inputs, sgate_w[...]), dot(inputs, sup_w[...]))
-    shared_out[...] = dot(
-        shared_hidden, sdown_w[:, pl.ds(pl.multiple_of(other * half, half), half)]
-    ).astype(BF16)
-    shared_copy = remote(shared_out, shared_in, shared_sem.at[0], shared_sem.at[1], ep, other)
-    shared_copy.start()
-    shared_own = dot(shared_hidden, sdown_w[:, pl.ds(pl.multiple_of(tp * half, half), half)])
-
-    for d in range(1, outer):
-        j = lax.rem(z + d, outer)
-        remote(
-            column.at[j], column.at[j], col_send.at[j], col_recv.at[j], ep, tp
-        ).wait_recv()
-        dispatch(j)
-
-    for load in loads[3:]:
-        load.wait()
-
-    pair_copies = []
-    for d in range(outer):
-        j = lax.rem(z + d, outer)
-        for e in range(1, inner):
-            source = lax.rem(p + e, inner)
-            remote(
-                staged.at[j, source],
-                rows_in.at[tp, j, source],
-                plane_send.at[j, source],
-                plane_recv.at[j, source],
-                ep,
-                tp,
-            ).wait_recv()
-        copy = remote(
-            rows_in.at[tp, j], rows_in.at[tp, j], pair_send.at[j], pair_recv.at[j], ep, other
-        )
-        copy.start()
-        pair_copies.append(copy)
-
-    total = experts * cap
-
-    def half_rows(which):
-        return pl.ds(pl.multiple_of(which * half, half), half)
-
-    own_rows = rows_in[tp].reshape(total, half)
-    gate_acc[...] = dot(own_rows, gate_w[half_rows(tp), :])
-    up_acc[...] = dot(own_rows, up_w[half_rows(tp), :])
-    for d in range(outer):
-        j = lax.rem(z + d, outer)
-        remote(
-            rows_in.at[other, j], rows_in.at[other, j], pair_send.at[j], pair_recv.at[j], ep, other
-        ).wait_recv()
-    other_rows = rows_in[other].reshape(total, half)
-    gate_value = gate_acc[...] + dot(other_rows, gate_w[half_rows(other), :])
-    upward = up_acc[...] + dot(other_rows, up_w[half_rows(other), :])
-    hidden = silu_product(gate_value, upward)
-
-    part_out[...] = (
-        dot(hidden, down_w[:, half_rows(other)]).astype(BF16).reshape(outer, inner, cap, half)
-    )
-    for d in range(outer):
-        j = lax.rem(z + 1 + d, outer)
-        copy = remote(part_out.at[j], part_in.at[j], part_send.at[j], part_recv.at[j], ep, other)
-        copy.start()
-        sends.append(copy)
-    part_own[...] = (
-        dot(hidden, down_w[:, half_rows(tp)]).astype(BF16).reshape(outer, inner, cap, half)
-    )
-
-    for d in range(outer):
-        j = lax.rem(z + 1 + d, outer)
-        remote(
-            part_out.at[j], part_in.at[j], part_send.at[j], part_recv.at[j], ep, other
-        ).wait_recv()
-        summed = part_own[j].astype(F32) + part_in[j].astype(F32)
-        result[j] = summed.astype(BF16)
-        for e in range(1, inner):
-            to = lax.rem(p + e, inner)
-            copy = remote(
+    def pair(i):
+        j = order[i]
+        for source in peers:
+            arrive(rows_in.at[tp, j, source], plane_send.at[j, source], plane_recv.at[j, source])
+        here = rows_in.at[tp, j]
+        send(here, here, pair_send.at[j], pair_recv.at[j], ep, other)
+
+    def expert(group):
+        if group[0] == 0:
+            for load in loads[3:]:
+                load.wait()
+
+        def rows_of(which):
+            blocks = [rows_in[which, order[i]].reshape(slots, half) for i in group]
+            return jnp.concatenate(blocks, axis=0)
+
+        own_rows = rows_of(tp)
+        gate_value = dot(own_rows, gate_w[half_of(tp), :])
+        upward = dot(own_rows, up_w[half_of(tp), :])
+        for i in group:
+            j = order[i]
+            arrive(rows_in.at[other, j], pair_send.at[j], pair_recv.at[j])
+        other_rows = rows_of(other)
+        gate_value = gate_value + dot(other_rows, gate_w[half_of(other), :])
+        upward = upward + dot(other_rows, up_w[half_of(other), :])
+        hidden = silu_product(gate_value, upward)
+
+        def store(target, values):
+            for n, i in enumerate(group):
+                block = values[n * slots : (n + 1) * slots]
+                target[order[i]] = block.astype(BF16).reshape(inner, cap, half)
+
+        store(part_out, dot(hidden, down_w[:, half_of(other)]))
+        for i in reversed(group):
+            j = order[i]
+            send(part_out.at[j], part_in.at[j], part_send.at[j], part_recv.at[j], ep, other)
+        store(part_own, dot(hidden, down_w[:, half_of(tp)]))
+
+    def give_back(i):
+        j = order[i]
+        arrive(part_in.at[j], part_send.at[j], part_recv.at[j])
+        result[j] = (part_own[j].astype(F32) + part_in[j].astype(F32)).astype(BF16)
+        for to in peers:
+            send(
                 result.at[j, to],
                 back.at[j, p],
                 back_send.at[j, to],
@@ -291,50 +295,59 @@
                 z * inner + to,
                 tp,
             )
-            copy.start()
-            sends.append(copy)
         back[j, p] = result[j, p]
 
-    pick_high = selector(experts)
-    pick_low = selector(2 * experts)
-    slot_of_lane = (lax.broadcasted_iota(jnp.int32, (local_tokens, slots), 1) % cap + 1).astype(F32)
-
-    def combine(j):
+    def combine(i):
+        j = order[i]
         facts = column[j, :, half:]
         chosen = dot_t(facts, pick_place) == slot_of_lane
         high_part = jnp.where(chosen, dot_t(facts, pick_high), 0.0).astype(BF16)
         low_part = jnp.where(chosen, dot_t(facts, pick_low), 0.0).astype(BF16)
-        for e in range(1, inner):
-            source = lax.rem(p + e, inner)
-            remote(
-                result.at[j, source],
-                back.at[j, source],
-                back_send.at[j, source],
-                back_recv.at[j, source],
-                ep,
-                tp,
-            ).wait_recv()
+        for source in peers:
+            arrive(back.at[j, source], back_send.at[j, source], back_recv.at[j, source])
         values = back[j].reshape(slots, half)
         return dot(high_part, values) + dot(low_part, values)
 
-    for d in range(1, outer):
-        j = lax.rem(z + d, outer)
-        sum_out[j] = combine(j).astype(BF16)
-        copy = remote(
-            sum_out.at[j], sum_in.at[z], sum_send.at[j], sum_recv.at[z], j * inner + p, tp
-        )
-        copy.start()
-        sends.append(copy)
-    combined = combine(z)
-    shared_copy.wait_recv()
-    combined = combined + (
-        shared_own.astype(BF16).astype(F32) + shared_in[...].astype(F32)
-    ).astype(BF16).astype(F32)
-    for d in range(1, outer):
-        j = lax.rem(z + d, outer)
-        remote(
-            sum_out.at[j], sum_in.at[j], sum_send.at[j], sum_recv.at[j], ep, tp
-        ).wait_recv()
+    dispatch(0)
+
+    for load in loads[:3]:
+        load.wait()
+    inputs = normed[...]
+    shared_hidden = silu_product(dot(inputs, sgate_w[...]), dot(inputs, sup_w[...]))
+    shared_out[...] = dot(shared_hidden, sdown_w[:, half_of(other)]).astype(BF16)
+    send(shared_out, shared_in, shared_sem.at[0], shared_sem.at[1], ep, other)
+    shared_own = dot(shared_hidden, sdown_w[:, half_of(tp)]).astype(BF16)
+
+    def step(task, what):
+        with jax.named_scope(task.__name__ + str(what)):
+            task(what)
+
+    paired = 0
+    for i in range(1, outer):
+        step(dispatch, i)
+        if i < outer - 1:
+            step(pair, paired)
+            paired += 1
+    for group in [[i, i + 1] for i in range(0, outer, 2)]:
+        while paired <= group[-1]:
+            step(pair, paired)
+            paired += 1
+        step(expert, group)
+        for i in reversed(group):
+            step(give_back, i)
+
+    for i in [1] + list(range(outer - 1, 1, -1)):
+        j = order[i]
+        with jax.named_scope("combine" + str(i)):
+            sum_out[j] = combine(i).astype(BF16)
+            send(sum_out.at[j], sum_in.at[z], sum_send.at[j], sum_recv.at[z], j * inner + p, tp)
+    with jax.named_scope("combine0"):
+        combined = combine(0)
+        arrive(shared_in, shared_sem.at[0], shared_sem.at[1])
+        shared_rows = (shared_own.astype(F32) + shared_in[...].astype(F32)).astype(BF16)
+        combined = combined + shared_rows.astype(F32)
+    for j in order[1:]:
+        arrive(sum_in.at[j], sum_send.at[j], sum_recv.at[j])
         combined = combined + sum_in[j].astype(F32)
 
     own_squares = jnp.sum(combined * combined, axis=1, keepdims=True)
@@ -346,11 +359,20 @@
     scaled = combined * lax.rsqrt(squares / width + EPSILON)
     mixed[...] = (scaled * out_gain[...].astype(F32)[None, :]).astype(BF16)
 
+    for to in order[1:]:
+
+        @pl.when(direct(to))
+        def _(to=to):
+            column_copy(z, to, col_send.at[to]).wait_send()
+
+        on, wanted = passes(to)
+
+        @pl.when(wanted)
+        def _(to=to, on=on):
+            column_copy(to, on, col_pass.at[to]).wait_send()
+
     for copy in sends:
         copy.wait_send()
-    for copy in pair_copies:
-        copy.wait_send()
-    shared_copy.wait_send()
     sq_copy.wait_send()
 
 
@@ -380,7 +402,6 @@
     info_width = -(-3 * experts // 128) * 128
     hidden = gate_weight.shape[2]
     shared_width = shared_gate.shape[1]
-    total = experts * cap
 
     def vm(shape, kind=BF16):
         return pltpu.VMEM(shape, kind)
@@ -405,8 +426,6 @@
             vm((outer, local_tokens, half + info_width)),
             vm(grid_rows),
             vm((2,) + grid_rows),
-            vm((total, hidden), F32),
-            vm((total, hidden), F32),
             vm(grid_rows),
             vm(grid_rows),
             vm(grid_rows),
@@ -419,6 +438,7 @@
             vm((local_tokens, 128), F32),
             vm((local_tokens, 128), F32),
             dma((6,)),
+            dma((outer,)),
             dma((outer,)),
             dma((outer,)),
             dma((outer, inner)),

time: 37.6 us -> 35.2 us (0.936)
  Pallas kernels: 35.9 us -> 33.5 us
    pallas_call x1, Pallas kernels: 35.9 us -> 33.5 us  [body(): pl.pallas_call(functools.partial(kernel, outer, inner, cap, info_width),...]
where the time goes in v3:
time: 35.2 us; the launch traced here: 35 us
  Pallas kernels  33.5 us (95%)
  local copies, waits for them, and re-layouts  1.47 us (4%)
    pallas_call x1, Pallas kernels, body(): pl.pallas_call(functools.partial(kernel, outer, inner, cap, info_width),...  33.5 us
    unnamed x1, local copies, waits for them, and re-layouts  1.47 us

profile of v3, /device:TPU:1, one launch (start us, length us, event | category | flops | bytes accessed | tf_op | source)
XLA Modules:
  0.0 35.0 jit_solution(5239846591788643288)
XLA Ops:
  0.0 33.5 %shard_map.109 = bf16[32,1024]{1,0:T(8,128)(2,1)} custom-call(bf16[32,2048]{1,0:T(8,128)(2,1)} %tokens.1, bf16[2048]{0:T(1024)(128)(2,1)} %in_gain.1, s32[6,32]{1,0:T(8,128)} %bitcast.2, f32[6,32]{1,0:T(8,128)} %bitcast.3, bf16[1024]{0:T(1024)(128)(2,1)} %out_gain.1, bf16[1,2048,384]{2,1,0:T(8,128)(2,1)} %gate_hbm.1, bf16[1,2048,384]{2,1,0:T(8,128)(2,1)} %up_hbm.1, ...), custom_call_target="tpu_custom_call" | custom-call | tf_op jit(solution)/shard_map/pallas_call | solution.py:413
  33.5 1.5 %copy.13 = bf16[32,1024]{1,0:T(8,128)(2,1)} copy(bf16[32,1024]{1,0:T(8,128)(2,1)} %shard_map.109) | data formatting | bytes 131072

commit v4 on v3

--- a/solution.py
+++ b/solution.py
@@ -29,11 +29,11 @@
     inner,
     cap,
     info_width,
-    tokens,
-    in_gain,
-    route_expert,
-    route_weight,
-    out_gain,
+    tokens_hbm,
+    in_gain_hbm,
+    route_expert_hbm,
+    route_weight_hbm,
+    out_gain_hbm,
     gate_hbm,
     up_hbm,
     down_hbm,
@@ -41,6 +41,11 @@
     sup_hbm,
     sdown_hbm,
     mixed,
+    tokens,
+    in_gain,
+    route_expert,
+    route_weight,
+    out_gain,
     gate_w,
     up_w,
     down_w,
@@ -92,6 +97,11 @@
         pltpu.make_async_copy(src, dst, w_sem.at[i])
         for i, (src, dst) in enumerate(
             [
+                (tokens_hbm, tokens),
+                (in_gain_hbm, in_gain),
+                (route_expert_hbm, route_expert),
+                (route_weight_hbm, route_weight),
+                (out_gain_hbm, out_gain),
                 (sgate_hbm, sgate_w),
                 (sup_hbm, sup_w),
                 (sdown_hbm, sdown_w),
@@ -101,7 +111,7 @@
             ]
         )
     ]
-    for load in loads:
+    for load in loads[:5]:
         load.start()
 
     barrier = pltpu.get_barrier_semaphore()
@@ -127,6 +137,10 @@
             device_id_type=pl.DeviceIdType.MESH,
         )
 
+    for load in loads[:5]:
+        load.wait()
+    for load in loads[5:]:
+        load.start()
     floats = tokens[...].astype(F32)
     mean = jnp.sum(floats * floats, axis=1, keepdims=True) / width
     rows = (floats * lax.rsqrt(mean + EPSILON) * in_gain[...].astype(F32)[None, :]).astype(BF16)
@@ -253,7 +267,7 @@
 
     def expert(group):
         if group[0] == 0:
-            for load in loads[3:]:
+            for load in loads[8:]:
                 load.wait()
 
         def rows_of(which):
@@ -310,7 +324,7 @@
 
     dispatch(0)
 
-    for load in loads[:3]:
+    for load in loads[5:8]:
         load.wait()
     inputs = normed[...]
     shared_hidden = silu_product(dot(inputs, sgate_w[...]), dot(inputs, sup_w[...]))
@@ -322,19 +336,18 @@
         with jax.named_scope(task.__name__ + str(what)):
             task(what)
 
-    paired = 0
     for i in range(1, outer):
         step(dispatch, i)
-        if i < outer - 1:
-            step(pair, paired)
-            paired += 1
-    for group in [[i, i + 1] for i in range(0, outer, 2)]:
-        while paired <= group[-1]:
-            step(pair, paired)
-            paired += 1
-        step(expert, group)
-        for i in reversed(group):
-            step(give_back, i)
+        if i == 1:
+            step(pair, 0)
+    step(pair, 1)
+    for first in range(0, outer, 2):
+        step(expert, (first, first + 1))
+        if first + 2 < outer:
+            step(pair, first + 2)
+            step(pair, first + 3)
+        step(give_back, first + 1)
+        step(give_back, first)
 
     for i in [1] + list(range(outer - 1, 1, -1)):
         j = order[i]
@@ -413,9 +426,14 @@
     return pl.pallas_call(
         functools.partial(kernel, outer, inner, cap, info_width),
         out_shape=jax.ShapeDtypeStruct((local_tokens, half), BF16),
-        in_specs=[in_vmem] * 5 + [anywhere] * 6,
+        in_specs=[anywhere] * 11,
         out_specs=in_vmem,
         scratch_shapes=[
+            vm((local_tokens, width)),
+            vm((width,)),
+            vm((top_count, local_tokens), jnp.int32),
+            vm((top_count, local_tokens), F32),
+            vm((half,)),
             vm((width, hidden)),
             vm((width, hidden)),
             vm((hidden, width)),
@@ -437,7 +455,7 @@
             vm((local_tokens, half)),
             vm((local_tokens, 128), F32),
             vm((local_tokens, 128), F32),
-            dma((6,)),
+            dma((11,)),
             dma((outer,)),
             dma((outer,)),
             dma((outer,)),

time: 35.2 us -> 34 us (0.966)
  Pallas kernels: 33.5 us -> 32.3 us
    pallas_call x1, Pallas kernels: 33.5 us -> 32.3 us  [body(): pl.pallas_call(functools.partial(kernel, outer, inner, cap, info_width),...]
where the time goes in v4:
time: 34 us; the launch traced here: 33.8 us
  Pallas kernels  32.3 us (95%)
  local copies, waits for them, and re-layouts  1.47 us (4%)
    pallas_call x1, Pallas kernels, body(): pl.pallas_call(functools.partial(kernel, outer, inner, cap, info_width),...  32.3 us
    unnamed x1, local copies, waits for them, and re-layouts  1.47 us

profile of v4, /device:TPU:1, one launch (start us, length us, event | category | flops | bytes accessed | tf_op | source)
XLA Modules:
  0.0 33.8 jit_solution(2327113619095275704)
XLA Ops:
  0.0 32.3 %shard_map.109 = bf16[32,1024]{1,0:T(8,128)(2,1)} custom-call(bf16[32,2048]{1,0:T(8,128)(2,1)} %tokens_hbm.1, bf16[2048]{0:T(1024)(128)(2,1)} %in_gain_hbm.1, s32[6,32]{1,0:T(8,128)} %bitcast.2, f32[6,32]{1,0:T(8,128)} %bitcast.3, bf16[1024]{0:T(1024)(128)(2,1)} %out_gain_hbm.1, bf16[1,2048,384]{2,1,0:T(8,128)(2,1)} %gate_hbm.1, ...), custom_call_target="tpu_custom_call" | custom-call | tf_op jit(solution)/shard_map/pallas_call | solution.py:426
  32.3 1.5 %copy.13 = bf16[32,1024]{1,0:T(8,128)(2,1)} copy(bf16[32,1024]{1,0:T(8,128)(2,1)} %shard_map.109) | data formatting | bytes 131072
